TPU v7x, 32 devices: a whole 2x2x4 slice. The times are simulated.
32 devices in a mesh: sp: 4 (over y, x), tp: 8 (over z, core).
Axes of the slice: x: 2, y: 2, z: 4, core: 2. Of those that a mesh axis runs over, the one named last changes fastest.
Arguments:
- tokens: bfloat16 [8192, 2048], P('sp', 'tp'), may hold values from -6 to 6
- norm_gain: float32 [2048], replicated, may hold values from 0.1 to 1.9
- w_key: bfloat16 [2048, 1024], P(None, 'tp'), may hold values from -0.125 to 0.125
- w_decay: bfloat16 [2048, 1024], P(None, 'tp'), may hold values from -0.125 to 0.125
- w_value: bfloat16 [2048, 512], replicated, may hold values from -0.125 to 0.125
- decay_bias: float32 [1024], P('tp'), may hold values from 0 to 8.5
- gate_drift: float32 [8192], P('sp'), may hold values from -1 to 1
- queries: bfloat16 [1024], P('tp'), may hold values from -6 to 6
- out_gain: float32 [4, 512], P(None, 'sp'), may hold values from 0.1 to 1.9
Outputs:
- state_cache: bfloat16 [1024, 512], P('tp', 'sp')
- first_read: float32 [4, 512], P(None, 'sp')
All inputs are finite; a program needn't handle non-finite values.
Results may differ from a plain program's by a relative error of at most 0.009.
Values may be sent and summed in bfloat16 or wider, within the bound.
A program may use at most 128 MiB of HBM per device.

v0:
```python
import jax
import jax.numpy as jnp
from jax import lax
from jax.sharding import PartitionSpec as P

QUERY_KEY_HEADS = 4
KEY_CHANNELS = 256
VALUE_CHANNELS = 512
EPS = 1e-06
GATE_NORM = 16.0


def body(tokens, norm_gain, w_key, w_decay, w_value, decay_bias, gate_drift, queries, out_gain):
    gathered = lax.all_gather(tokens, "tp", axis=1, tiled=True)
    rows_f32 = gathered.astype(jnp.float32)
    inverse_rms = lax.rsqrt(jnp.mean(rows_f32 * rows_f32, axis=1, keepdims=True) + EPS)
    normed = (rows_f32 * inverse_rms * norm_gain[None, :]).astype(jnp.bfloat16)
    key_proj = jnp.dot(normed, w_key, preferred_element_type=jnp.float32).astype(jnp.bfloat16)
    gate_pre = jnp.dot(normed, w_decay, preferred_element_type=jnp.float32).astype(jnp.bfloat16)
    value_proj = jnp.dot(normed, w_value, preferred_element_type=jnp.float32).astype(jnp.bfloat16)
    log_decay = (
        jax.nn.log_sigmoid(gate_pre.astype(jnp.float32) + decay_bias[None, :] + gate_drift[:, None])
        / GATE_NORM
    )
    suffix = lax.cumsum(log_decay, axis=0, reverse=True)
    weighted = (key_proj.astype(jnp.float32) * jnp.exp(suffix - log_decay)).astype(jnp.bfloat16)
    partial_value = lax.dot_general(
        weighted, value_proj, (((0,), (0,)), ((), ())), preferred_element_type=jnp.float32
    )
    total_decay = suffix[0]
    channels = partial_value.shape[0]
    span_count = lax.axis_size("sp")
    spread = jnp.broadcast_to(total_decay[None, :, None], (1, channels, span_count))
    blocks, totals = (
        lax.all_to_all(partial_value[None], "sp", split_axis=2, concat_axis=0, tiled=True),
        lax.all_to_all(spread, "sp", split_axis=2, concat_axis=0, tiled=True),
    )
    later_sum = lax.cumsum(totals, axis=0, reverse=True) - totals
    matrix_state = jnp.sum(jnp.exp(later_sum) * blocks, axis=0)
    state_cache = matrix_state.astype(jnp.bfloat16)
    channel_ids = lax.axis_index("tp") * channels + jnp.arange(channels, dtype=jnp.int32)
    owners = (channel_ids // KEY_CHANNELS)[:, None] == jnp.arange(QUERY_KEY_HEADS, dtype=jnp.int32)[
        None, :
    ]
    query_of_head = jnp.where(
        owners, queries.astype(jnp.float32)[:, None] * KEY_CHANNELS ** (-0.5), 0.0
    )
    part_read = lax.dot_general(
        query_of_head, matrix_state, (((0,), (0,)), ((), ())), precision=lax.Precision.HIGHEST
    )
    summed_read = lax.psum(part_read, "tp")
    squares = lax.psum(jnp.sum(summed_read * summed_read, axis=1), "sp")
    first_read = summed_read * lax.rsqrt(squares / VALUE_CHANNELS + EPS)[:, None] * out_gain
    return (state_cache, first_read)


def solution(mesh):
    return jax.shard_map(
        body,
        mesh=mesh,
        in_specs=(
            P("sp", "tp"),
            P(),
            P(None, "tp"),
            P(None, "tp"),
            P(),
            P("tp"),
            P("sp"),
            P("tp"),
            P(None, "sp"),
        ),
        out_specs=(P("tp", "sp"), P(None, "sp")),
        check_vma=False,
    )
```

profile of v0, /device:TPU:0, one launch (start us, length us, event | category | flops | bytes accessed | tf_op | source)
XLA Modules:
  0.0 171.0 jit_solution(2722808447826279931)
XLA Ops:
  7.2 0.0 copy-start
  7.2 0.0 copy-start.5
  7.2 0.0 copy-start.3
  7.2 0.0 copy-start.6
  7.2 0.0 copy-start.4
  7.2 0.0 all-gather.2.cloned.1.call-start
  7.3 0.7 all-gather.2.cloned.1.call-update
  8.0 0.7 convert_multiply_fusion.2
  8.7 86.2 %all-gather.2.cloned.1.call-done = bf16[2048,2048]{1,0:T(8,128)(2,1)} async-done(((bf16[2048,256]{1,0:T(8,128)(2,1)}), bf16[2048,2048]{1,0:T(8,128)(2,1)}) %all-gather.2.cloned.1.call-update) | async-done | bytes 8388624 | tf_op jit(solution)/shard_map/all_gather | solution.py:14
  94.9 0.0 copy-start.1
  94.9 5.2 %fusion = f32[2048]{0:T(1024)S(1)} fusion(bf16[2048,2048]{1,0:T(8,128)(2,1)} %all-gather.2.cloned.1.call-done), kind=kLoop, calls=%fused_computation.2 | loop fusion | flops 12580864 | bytes 8396800 | tf_op jit(solution)/shard_map/reduce_sum | solution.py:16
  100.1 0.0 copy-done.5
  100.1 0.0 copy-done.3
  100.1 0.0 copy-done.6
  100.1 0.0 copy-done.4
  100.1 0.5 copy-done.1
  100.6 4.7 %fusion.12 = (f32[128,2048]{0,1:T(8,128)S(1)}, f32[2048,128]{1,0:T(8,128)}) fusion(f32[2048]{0:T(1024)S(1)} %copy-done.4, f32[128]{0:T(128)S(1)} %copy-done.6, bf16[2048,128]{1,0:T(8,128)(2,1)S(1)} %copy-done.3, bf16[2048,2048]{1,0:T(8,128)(2,1)S(1)} %copy-done.1, f32[2048]{0:T(1024)S(1)} %copy-done.5, f32[2048]{0:T(1024)S(1)} %add_rsqrt_fusion), kind=kOutput, calls=%fused_computation.19 | convolution fusion | flops 1093926912 | bytes 11035136 | tf_op jit(solution)/shard_map/dot_general | solution.py:19
  105.4 2.6 %fusion.21 = f32[128,16,128]{0,1,2:T(8,128)S(1)} fusion(f32[128,16,128]{0,2,1:T(8,128)S(1)} %bitcast.44), kind=kOutput, calls=%fused_computation.30 | output fusion | flops 33292288 | bytes 2097152 | tf_op jit(solution)/shard_map/reduce-window
  108.0 0.1 broadcast_add_fusion
  108.1 0.3 copy.17
  108.4 0.6 broadcast_in_dim.19
  109.0 3.6 %all-to-all-start = ((f32[1,128,4]{1,0,2:T(1,128)}), f32[1,128,4]{1,0,2:T(1,128)S(1)}, u32[]{:S(2)}, u32[]{:S(2)}) async-start(f32[1,128,4]{1,0,2:T(1,128)} %broadcast_in_dim.19), calls=%async_computation | async-start | bytes 4096 | tf_op jit(solution)/shard_map/all_to_all | solution.py:36
  112.6 7.6 %fusion.9 = bf16[2048,128]{1,0:T(8,128)(2,1)} fusion(bf16[2048,128]{1,0:T(8,128)(2,1)} %param.11, f32[2048,128]{1,0:T(8,128)S(1)} %bitcast.43, f32[2048,128]{1,0:T(8,128)} %get-tuple-element.5, bf16[2048,2048]{1,0:T(8,128)(2,1)} %all-gather.2.cloned.1.call-done, f32[2048]{0:T(1024)S(1)} %copy-done.5, f32[2048]{0:T(1024)S(1)} %add_rsqrt_fusion), kind=kOutput, calls=%fused_computation.16 | convolution fusion | flops 1093926912 | bytes 11550720 | tf_op jit(solution)/shard_map/dot_general | solution.py:18
  120.2 0.0 copy-done
  120.2 0.0 copy-start.2
  120.2 10.2 %fusion.10 = f32[128,512]{0,1:T(8,128)} fusion(bf16[2048,128]{1,0:T(8,128)(2,1)} %fusion.9, bf16[2048,512]{1,0:T(8,128)(2,1)S(1)} %copy-done, bf16[2048,2048]{1,0:T(8,128)(2,1)} %all-gather.2.cloned.1.call-done, f32[2048]{0:T(1024)S(1)} %copy-done.5, f32[2048]{0:T(1024)S(1)} %add_rsqrt_fusion), kind=kOutput, calls=%fused_computation.17 | convolution fusion | flops 4581228544 | bytes 11288576 | tf_op jit(solution)/shard_map/dot_general | solution.py:27
  130.4 0.0 all-to-all-done
  130.5 4.2 %all-to-all-start.1 = ((f32[1,128,512]{1,0,2:T(1,128)}), f32[1,128,512]{1,0,2:T(1,128)S(1)}, u32[]{:S(2)}, u32[]{:S(2)}) async-start(f32[1,128,512]{1,0,2:T(1,128)} %bitcast.18), calls=%async_computation.1 | async-start | bytes 524288 | tf_op jit(solution)/shard_map/all_to_all | solution.py:35
  134.7 5.3 %all-to-all-done.1 = f32[1,128,512]{1,0,2:T(1,128)S(1)} async-done(((f32[1,128,512]{1,0,2:T(1,128)}), f32[1,128,512]{1,0,2:T(1,128)S(1)}, u32[]{:S(2)}, u32[]{:S(2)}) %all-to-all-start.1) | async-done | bytes 262176 | tf_op jit(solution)/shard_map/all_to_all | solution.py:35
  140.0 0.3 fusion.23
  140.3 13.6 %psum.14 = f32[4,128]{1,0:T(4,128)S(1)} all-reduce(f32[4,128]{1,0:T(4,128)S(1)} %fusion.23), channel_id=1, replica_groups=mesh['sp'=4,'tp'=8] {'tp'}, use_global_device_ids=true, to_apply=%region_5.6 | all-reduce | flops 512 | bytes 4096 | tf_op jit(solution)/shard_map/psum | solution.py:51
  153.9 0.1 multiply_reduce_fusion.1
  154.1 8.7 %psum.15 = f32[4]{0:T(128)S(1)} all-reduce(f32[4]{0:T(128)S(1)} %multiply_reduce_fusion.1), channel_id=1, replica_groups=mesh['sp'=4,'tp'=8] {'sp'}, use_global_device_ids=true, to_apply=%region_7.8 | all-reduce | flops 4 | bytes 32 | tf_op jit(solution)/shard_map/psum | solution.py:52
  162.8 0.7 copy.19
  163.5 0.0 copy-done.2
  163.5 0.6 multiply_multiply_fusion
  (11 shorter events, 0.1 us)
Async XLA Ops:
  7.2 113.1 %copy-start = (bf16[2048,512]{1,0:T(8,128)(2,1)S(1)}, bf16[2048,512]{1,0:T(8,128)(2,1)}, u32[]{:S(2)}) copy-start(bf16[2048,512]{1,0:T(8,128)(2,1)} %param.13) | copy-start | bytes 6291460
  7.2 92.9 %copy-start.5 = (f32[2048]{0:T(1024)S(1)}, f32[2048]{0:T(1024)}, u32[]{:S(2)}) copy-start(f32[2048]{0:T(1024)} %param.10) | copy-start | bytes 24580
  7.2 92.9 %copy-start.3 = (bf16[2048,128]{1,0:T(8,128)(2,1)S(1)}, bf16[2048,128]{1,0:T(8,128)(2,1)}, u32[]{:S(2)}) copy-start(bf16[2048,128]{1,0:T(8,128)(2,1)} %param.12) | copy-start | bytes 1572868
  7.2 92.9 %copy-start.6 = (f32[128]{0:T(128)S(1)}, f32[128]{0:T(128)}, u32[]{:S(2)}) copy-start(f32[128]{0:T(128)} %param.14) | copy-start | bytes 1540
  7.2 92.9 %copy-start.4 = (f32[2048]{0:T(1024)S(1)}, f32[2048]{0:T(1024)}, u32[]{:S(2)}) copy-start(f32[2048]{0:T(1024)} %param.15) | copy-start | bytes 24580
  7.2 87.6 %all-gather.2.cloned.1.call-start = ((), (), s32[]{:S(2)}) async-start(), calls=%async_computation.2 | async-start | bytes 9437184 | tf_op jit(solution)/shard_map/all_gather | solution.py:14
  94.9 5.8 %copy-start.1 = (bf16[2048,2048]{1,0:T(8,128)(2,1)S(1)}, bf16[2048,2048]{1,0:T(8,128)(2,1)}, u32[]{:S(2)}) copy-start(bf16[2048,2048]{1,0:T(8,128)(2,1)} %all-gather.2.cloned.1.call-done) | copy-start | bytes 25165828
  109.0 21.5 %all-to-all-start = ((f32[1,128,4]{1,0,2:T(1,128)}), f32[1,128,4]{1,0,2:T(1,128)S(1)}, u32[]{:S(2)}, u32[]{:S(2)}) async-start(f32[1,128,4]{1,0,2:T(1,128)} %broadcast_in_dim.19), calls=%async_computation | async-start | bytes 4096 | tf_op jit(solution)/shard_map/all_to_all | solution.py:36
  120.2 43.3 %copy-start.2 = (f32[4,128]{1,0:T(4,128)S(1)}, f32[4,128]{1,0:T(4,128)}, u32[]{:S(2)}) copy-start(f32[4,128]{1,0:T(4,128)} %param.17) | copy-start | bytes 6148
  130.5 9.6 %all-to-all-start.1 = ((f32[1,128,512]{1,0,2:T(1,128)}), f32[1,128,512]{1,0,2:T(1,128)S(1)}, u32[]{:S(2)}, u32[]{:S(2)}) async-start(f32[1,128,512]{1,0,2:T(1,128)} %bitcast.18), calls=%async_computation.1 | async-start | bytes 524288 | tf_op jit(solution)/shard_map/all_to_all | solution.py:35
Sparse Core Ops, SparseCore 0:
  9.6 85.1 all-gather.1
where the time goes:
time: 171 us
  waiting for transfers between devices  92.2 us (54%)
  matrix products  22.8 us (13%)
  blocking collectives  22.4 us (13%)
  between operations  14.2 us (8%)
  other arithmetic  9.45 us (6%)
  starting transfers between devices  7.88 us (5%)
  local copies, waits for them, and re-layouts  2.17 us (1%)
    all_gather x1, waiting for transfers between devices, body(): gathered = lax.all_gather(tokens, 'tp', axis=1, tiled=True)  86.2 us
    psum x1, blocking collectives, body(): summed_read = lax.psum(part_read, 'tp')  13.6 us
    dot_general x1, matrix products, body(): lax.dot_general(weighted, value_proj, (((0,), (0,)), ((), ())), preferred...  10.2 us
    psum x1, blocking collectives, body(): squares = lax.psum(jnp.sum(summed_read * summed_read, axis=1), 'sp')  8.74 us
    dot_general x1, matrix products, body(): jnp.dot(normed, w_key, preferred_element_type=jnp.float32)  7.58 us
    all_to_all x1, waiting for transfers between devices, body(): lax.all_to_all(partial_value[None], 'sp', split_axis=2, concat_axis=0, ti...  5.33 us
    reduce_sum x1, other arithmetic, body(): jnp.mean(rows_f32 * rows_f32, axis=1, keepdims=True) + EPS  5.23 us
    dot_general x1, matrix products, body(): jnp.dot(normed, w_decay, preferred_element_type=jnp.float32)  4.74 us
  transfers between devices with their start and end apart: 3, of which 2 were waited for; matrix products, arithmetic and copies ran while one was open for 11% of the time, Pallas kernels for 0%

commit v1 on v0

--- a/solution.py
+++ b/solution.py
@@ -11,7 +11,15 @@
 
 
 def body(tokens, norm_gain, w_key, w_decay, w_value, decay_bias, gate_drift, queries, out_gain):
-    gathered = lax.all_gather(tokens, "tp", axis=1, tiled=True)
+    gathered = jnp.concatenate(
+        lax.all_to_all(
+            jnp.stack([tokens for _ in range(lax.axis_size("tp"))], 0),
+            "tp",
+            concat_axis=0,
+            split_axis=0,
+        ),
+        1,
+    )
     rows_f32 = gathered.astype(jnp.float32)
     inverse_rms = lax.rsqrt(jnp.mean(rows_f32 * rows_f32, axis=1, keepdims=True) + EPS)
     normed = (rows_f32 * inverse_rms * norm_gain[None, :]).astype(jnp.bfloat16)

time: 171 us -> 277 us (1.62)
  waiting for transfers between devices: 92.2 us -> 189 us
  between operations: 14.2 us -> 0.77 us
  other arithmetic: 9.45 us -> 17.2 us
  starting transfers between devices: 7.88 us -> 14.5 us
  local copies, waits for them, and re-layouts: 2.17 us -> 7.62 us
    all_to_all x0 -> x1, waiting for transfers between devices: none -> 184 us  [body(): lax.all_to_all(jnp.stack([tokens for _ in range(lax.axis_size('tp'))], 0)...]
    all_gather x1 -> x0, waiting for transfers between devices: 86.2 us -> none  [body(): gathered = lax.all_gather(tokens, 'tp', axis=1, tiled=True)]
    convert_element_type x0 -> x1, other arithmetic: none -> 8.58 us  [body(): normed = (rows_f32 * inverse_rms * norm_gain[None, :]).astype(jnp.bfloat16)]
    all_to_all x0 -> x1, starting transfers between devices: none -> 6.49 us  [body(): lax.all_to_all(jnp.stack([tokens for _ in range(lax.axis_size('tp'))], 0)...]
    another operation x2 -> x3, local copies, waits for them, and re-layouts: 0.01 us -> 4.29 us  [the longest x1 4.28 us: body(): jnp.stack([tokens for _ in range(lax.axis_size('tp'))], 0)]
    dot_general x1, matrix products: 4.74 us -> 7.51 us  [body(): jnp.dot(normed, w_decay, preferred_element_type=jnp.float32)]
  transfers between devices with their start and end apart: 3 -> 3, of which waited for: 2 -> 2; matrix products, arithmetic and copies ran while one was open for 11% -> 6% of each run, Pallas kernels for 0% -> 0%
where the time goes in v1:
time: 277 us
  waiting for transfers between devices  189 us (68%)
  matrix products  25.3 us (9%)
  blocking collectives  22.4 us (8%)
  other arithmetic  17.2 us (6%)
  starting transfers between devices  14.5 us (5%)
  local copies, waits for them, and re-layouts  7.62 us (3%)
    all_to_all x1, waiting for transfers between devices, body(): lax.all_to_all(jnp.stack([tokens for _ in range(lax.axis_size('tp'))], 0)...  184 us
    psum x1, blocking collectives, body(): summed_read = lax.psum(part_read, 'tp')  13.6 us
    dot_general x1, matrix products, body(): lax.dot_general(weighted, value_proj, (((0,), (0,)), ((), ())), preferred...  10.1 us
    psum x1, blocking collectives, body(): squares = lax.psum(jnp.sum(summed_read * summed_read, axis=1), 'sp')  8.74 us
    convert_element_type x1, other arithmetic, body(): normed = (rows_f32 * inverse_rms * norm_gain[None, :]).astype(jnp.bfloat16)  8.58 us
    dot_general x1, matrix products, body(): jnp.dot(normed, w_decay, preferred_element_type=jnp.float32)  7.51 us
    dot_general x1, matrix products, body(): jnp.dot(normed, w_key, preferred_element_type=jnp.float32)  7.37 us
    all_to_all x1, starting transfers between devices, body(): lax.all_to_all(jnp.stack([tokens for _ in range(lax.axis_size('tp'))], 0)...  6.49 us
  transfers between devices with their start and end apart: 3, of which 2 were waited for; matrix products, arithmetic and copies ran while one was open for 6% of the time, Pallas kernels for 0%

profile of v1, /device:TPU:0, one launch (start us, length us, event | category | flops | bytes accessed | tf_op | source)
XLA Modules:
  0.0 277.0 jit_solution(8849921225284389855)
XLA Ops:
  0.6 0.0 copy-start
  0.6 1.6 copy.20
  2.3 4.3 %stack.2 = bf16[8,2048,256]{1,2,0:T(8,128)(2,1)} broadcast(bf16[2048,256]{0,1:T(8,128)(2,1)S(1)} %copy.20), dimensions={1,2} | broadcast | bytes 9437184 | tf_op jit(solution)/shard_map/stack | solution.py:16
  6.6 0.0 copy-start.5
  6.6 6.5 %all-to-all-start = ((bf16[8,2048,256]{1,2,0:T(8,128)(2,1)}), bf16[8,2048,256]{1,2,0:T(8,128)(2,1)}, u32[]{:S(2)}, u32[]{:S(2)}) async-start(bf16[8,2048,256]{1,2,0:T(8,128)(2,1)} %stack.2), calls=%async_computation | async-start | bytes 16777216 | tf_op jit(solution)/shard_map/all_to_all | solution.py:15
  13.1 0.0 copy-start.1
  13.1 0.0 copy-done.5
  13.1 183.9 %all-to-all-done = bf16[8,2048,256]{1,2,0:T(8,128)(2,1)} async-done(((bf16[8,2048,256]{1,2,0:T(8,128)(2,1)}), bf16[8,2048,256]{1,2,0:T(8,128)(2,1)}, u32[]{:S(2)}, u32[]{:S(2)}) %all-to-all-start) | async-done | bytes 8388640 | tf_op jit(solution)/shard_map/all_to_all | solution.py:15
  197.0 5.1 %multiply_reduce_fusion = f32[2048]{0:T(1024)S(1)} fusion(bf16[8,2048,256]{1,2,0:T(8,128)(2,1)} %all-to-all-done), kind=kLoop, calls=%fused_computation.3 | loop fusion | flops 12580864 | bytes 8396800 | tf_op jit(solution)/shard_map/reduce_sum | solution.py:24
  202.1 0.0 copy-done.1
  202.2 0.0 copy-start.3
  202.2 0.0 copy-start.4
  202.2 0.0 copy-start.6
  202.2 8.6 %fusion.1 = bf16[2048,2048]{0,1:T(8,128)(2,1)} fusion(f32[2048]{0:T(1024)S(1)} %copy-done.1, f32[2048]{0:T(1024)S(1)} %add_rsqrt_fusion, bf16[8,2048,256]{1,2,0:T(8,128)(2,1)} %all-to-all-done), kind=kLoop, calls=%fused_computation.2 | loop fusion | flops 16777216 | bytes 16793600 | tf_op jit(solution)/shard_map/convert_element_type | solution.py:25
  210.8 0.0 copy-done.3
  210.8 0.0 copy-done.4
  210.8 0.0 copy-done.6
  210.8 7.5 %fusion.11 = (f32[128,2048]{0,1:T(8,128)S(1)}, f32[2048,128]{1,0:T(8,128)}) fusion(f32[2048]{0:T(1024)S(1)} %copy-done.4, f32[128]{0:T(128)S(1)} %copy-done.6, bf16[2048,2048]{0,1:T(8,128)(2,1)} %fusion.1, bf16[2048,128]{1,0:T(8,128)(2,1)S(1)} %copy-done.3), kind=kOutput, calls=%fused_computation.18 | convolution fusion | flops 1077149696 | bytes 11018752 | tf_op jit(solution)/shard_map/dot_general | solution.py:27
  218.3 2.6 fusion.20
  220.9 0.1 broadcast_add_fusion
  221.0 0.3 copy.22
  221.4 0.6 broadcast_in_dim.19
  221.9 3.8 %all-to-all-start.1 = ((f32[1,128,4]{1,0,2:T(1,128)}), f32[1,128,4]{1,0,2:T(1,128)S(1)}, u32[]{:S(2)}, u32[]{:S(2)}) async-start(f32[1,128,4]{1,0,2:T(1,128)} %broadcast_in_dim.19), calls=%async_computation.1 | async-start | bytes 4096 | tf_op jit(solution)/shard_map/all_to_all | solution.py:44
  225.7 7.4 %fusion.8 = bf16[2048,128]{1,0:T(8,128)(2,1)} fusion(bf16[2048,2048]{0,1:T(8,128)(2,1)} %fusion.1, bf16[2048,128]{1,0:T(8,128)(2,1)} %param.11, f32[2048,128]{1,0:T(8,128)S(1)} %bitcast.54, f32[2048,128]{1,0:T(8,128)} %get-tuple-element.5), kind=kOutput, calls=%fused_computation.15 | convolution fusion | flops 1077149696 | bytes 11534336 | tf_op jit(solution)/shard_map/dot_general | solution.py:26
  233.1 0.0 copy-done
  233.1 0.0 copy-start.2
  233.1 10.1 %fusion.9 = f32[128,512]{0,1:T(8,128)} fusion(bf16[2048,128]{1,0:T(8,128)(2,1)} %fusion.8, bf16[2048,2048]{0,1:T(8,128)(2,1)} %fusion.1, bf16[2048,512]{1,0:T(8,128)(2,1)S(1)} %copy-done), kind=kOutput, calls=%fused_computation.16 | convolution fusion | flops 4564451328 | bytes 11272192 | tf_op jit(solution)/shard_map/dot_general | solution.py:35
  243.2 0.0 all-to-all-done.1
  243.2 4.2 %all-to-all-start.2 = ((f32[1,128,512]{1,0,2:T(1,128)}), f32[1,128,512]{1,0,2:T(1,128)S(1)}, u32[]{:S(2)}, u32[]{:S(2)}) async-start(f32[1,128,512]{1,0,2:T(1,128)} %bitcast.21), calls=%async_computation.2 | async-start | bytes 524288 | tf_op jit(solution)/shard_map/all_to_all | solution.py:43
  247.5 5.3 %all-to-all-done.2 = f32[1,128,512]{1,0,2:T(1,128)S(1)} async-done(((f32[1,128,512]{1,0,2:T(1,128)}), f32[1,128,512]{1,0,2:T(1,128)S(1)}, u32[]{:S(2)}, u32[]{:S(2)}) %all-to-all-start.2) | async-done | bytes 262176 | tf_op jit(solution)/shard_map/all_to_all | solution.py:43
  252.8 0.3 fusion.22
  253.1 13.6 %psum.14 = f32[4,128]{1,0:T(4,128)S(1)} all-reduce(f32[4,128]{1,0:T(4,128)S(1)} %fusion.22), channel_id=1, replica_groups=mesh['sp'=4,'tp'=8] {'tp'}, use_global_device_ids=true, to_apply=%region_5.6 | all-reduce | flops 512 | bytes 4096 | tf_op jit(solution)/shard_map/psum | solution.py:59
  266.7 0.1 multiply_reduce_fusion.2
  266.8 8.7 %psum.15 = f32[4]{0:T(128)S(1)} all-reduce(f32[4]{0:T(128)S(1)} %multiply_reduce_fusion.2), channel_id=1, replica_groups=mesh['sp'=4,'tp'=8] {'sp'}, use_global_device_ids=true, to_apply=%region_7.8 | all-reduce | flops 4 | bytes 32 | tf_op jit(solution)/shard_map/psum | solution.py:60
  275.6 0.7 copy.24
  276.3 0.0 copy-done.2
  276.3 0.6 multiply_multiply_fusion
  (12 shorter events, 0.2 us)
Async XLA Ops:
  0.6 232.5 %copy-start = (bf16[2048,512]{1,0:T(8,128)(2,1)S(1)}, bf16[2048,512]{1,0:T(8,128)(2,1)}, u32[]{:S(2)}) copy-start(bf16[2048,512]{1,0:T(8,128)(2,1)} %param.13) | copy-start | bytes 6291460
  6.6 6.5 %copy-start.5 = (bf16[128]{0:T(256)(128)(2,1)S(1)}, bf16[128]{0:T(256)(128)(2,1)}, u32[]{:S(2)}) copy-start(bf16[128]{0:T(256)(128)(2,1)} %param.16) | copy-start | bytes 772
  6.6 190.4 %all-to-all-start = ((bf16[8,2048,256]{1,2,0:T(8,128)(2,1)}), bf16[8,2048,256]{1,2,0:T(8,128)(2,1)}, u32[]{:S(2)}, u32[]{:S(2)}) async-start(bf16[8,2048,256]{1,2,0:T(8,128)(2,1)} %stack.2), calls=%async_computation | async-start | bytes 16777216 | tf_op jit(solution)/shard_map/all_to_all | solution.py:15
  13.1 189.1 %copy-start.1 = (f32[2048]{0:T(1024)S(1)}, f32[2048]{0:T(1024)}, u32[]{:S(2)}) copy-start(f32[2048]{0:T(1024)} %param.10) | copy-start | bytes 24580
  202.2 8.6 %copy-start.3 = (bf16[2048,128]{1,0:T(8,128)(2,1)S(1)}, bf16[2048,128]{1,0:T(8,128)(2,1)}, u32[]{:S(2)}) copy-start(bf16[2048,128]{1,0:T(8,128)(2,1)} %param.12) | copy-start | bytes 1572868
  202.2 8.6 %copy-start.4 = (f32[2048]{0:T(1024)S(1)}, f32[2048]{0:T(1024)}, u32[]{:S(2)}) copy-start(f32[2048]{0:T(1024)} %param.15) | copy-start | bytes 24580
  202.2 8.6 %copy-start.6 = (f32[128]{0:T(128)S(1)}, f32[128]{0:T(128)}, u32[]{:S(2)}) copy-start(f32[128]{0:T(128)} %param.14) | copy-start | bytes 1540
  221.9 21.3 %all-to-all-start.1 = ((f32[1,128,4]{1,0,2:T(1,128)}), f32[1,128,4]{1,0,2:T(1,128)S(1)}, u32[]{:S(2)}, u32[]{:S(2)}) async-start(f32[1,128,4]{1,0,2:T(1,128)} %broadcast_in_dim.19), calls=%async_computation.1 | async-start | bytes 4096 | tf_op jit(solution)/shard_map/all_to_all | solution.py:44
  233.1 43.2 %copy-start.2 = (f32[4,128]{1,0:T(4,128)S(1)}, f32[4,128]{1,0:T(4,128)}, u32[]{:S(2)}) copy-start(f32[4,128]{1,0:T(4,128)} %param.17) | copy-start | bytes 6148
  243.2 9.6 %all-to-all-start.2 = ((f32[1,128,512]{1,0,2:T(1,128)}), f32[1,128,512]{1,0,2:T(1,128)S(1)}, u32[]{:S(2)}, u32[]{:S(2)}) async-start(f32[1,128,512]{1,0,2:T(1,128)} %bitcast.21), calls=%async_computation.2 | async-start | bytes 524288 | tf_op jit(solution)/shard_map/all_to_all | solution.py:43
